TPU v7x, 32 devices: a whole 2x2x4 slice. The times are simulated.
32 devices in a mesh: kv: 8 (over z, y), tp: 4 (over x, core).
Axes of the slice: x: 2, y: 2, z: 4, core: 2. Of those that a mesh axis runs over, the one named last changes fastest.
Arguments:
- tokens: bfloat16 [16, 16, 4096], replicated, may hold values from -6 to 6
- gain_pre: float32 [4096], replicated, may hold values from 0.1 to 1.9
- w_query: bfloat16 [4096, 2048], P('kv', 'tp'), may hold values from -0.09375 to 0.09375
- w_key: bfloat16 [4096, 2048], P('kv', 'tp'), may hold values from -0.09375 to 0.09375
- w_value: bfloat16 [4096, 2048], P('kv', 'tp'), may hold values from -0.09375 to 0.09375
- w_forget: bfloat16 [4096, 16], replicated, may hold values from -0.09375 to 0.09375
- b_forget: float32 [16], replicated
- w_out: bfloat16 [2048, 4096], P('tp', 'kv'), may hold values from -0.125 to 0.125
- gain_post: float32 [4096], P(('kv', 'tp')), may hold values from 0.1 to 1.9
- key_cache: bfloat16 [16, 1024, 16, 128], P(None, 'kv', 'tp'), may hold values from -6 to 6
- value_cache: bfloat16 [16, 1024, 16, 128], P(None, 'kv', 'tp'), may hold values from -6 to 6
- cum_cache: float32 [16, 1024, 16], P(None, 'kv', 'tp'), may hold values from -402 to 0, as said below
- lengths: int32 [16], replicated, may hold values from 512 to 992
- accepted: int32 [16], replicated, may hold values from 0 to 16
- parent: int32 [16, 16], replicated, may hold values from -1 to 14, as said below
Outputs:
- mixed: bfloat16 [16, 16, 4096], P(None, None, ('kv', 'tp'))
- key_out: bfloat16 [16, 1024, 16, 128], P(None, 'kv', 'tp')
- value_out: bfloat16 [16, 1024, 16, 128], P(None, 'kv', 'tp')
- cum_out: float32 [16, 1024, 16], P(None, 'kv', 'tp')
Inputs may be any that keep to these rules, and one draw needn't show every extreme that they name: parent[s, 0] is -1 and parent[s, i] lies between -1 and i - 1. `cum_cache`: along the positions of each sequence and head the values never rise. lengths + accepted + 16 never exceeds 1024.
All inputs are finite; a program needn't handle non-finite values.
Results may differ from a plain program's by a relative error of at most 0.03.
Values may be sent and summed in bfloat16 or wider, within the bound.
No kernel may reach another device: no remote copies, remote signals or barrier semaphores. Data moves between devices by JAX's collectives and lax.ppermute only.
A program may use at most 64 MiB of HBM per device.

v0:
```python
import jax
import jax.numpy as jnp
from jax import lax
from jax.experimental import pallas as pl
from jax.experimental.pallas import tpu as pltpu
from jax.sharding import PartitionSpec as P

epsilon = 1e-06
floor_value = -1e30


def split_float(x):
    high = lax.reduce_precision(x, 8, 7)
    rest = x - high
    middle = lax.reduce_precision(rest, 8, 7)
    low = rest - middle
    return [part.astype(jnp.bfloat16) for part in (high, middle, low)]


def pack_lanes(x, lanes):
    parts = jnp.concatenate(split_float(x), axis=-1)
    return jnp.pad(parts, ((0, 0), (0, lanes - parts.shape[-1])))


def unpack_lanes(packed, count):
    wide = packed.astype(jnp.float32)
    return (
        wide[..., :count] + wide[..., count : 2 * count] + wide[..., 2 * count : 3 * count]
    )


def gather_rows(rows, axis):
    size = lax.axis_size(axis)
    copies = jnp.broadcast_to(rows[None], (size,) + rows.shape)
    return lax.all_to_all(copies, axis, 0, 0, tiled=True).reshape(
        (size * rows.shape[0],) + rows.shape[1:]
    )


def exchange(rows, axis):
    size = lax.axis_size(axis)
    blocks = rows.reshape((size, rows.shape[0] // size) + rows.shape[1:])
    return lax.all_to_all(blocks, axis, 0, 0, tiled=True)


def shifted(block, axis, step):
    size = lax.axis_size(axis)
    return lax.ppermute(block, axis, [(i, (i + step) % size) for i in range(size)])


def fold_of(axis):
    return 2 if lax.axis_size(axis) % 2 == 0 else 1


def fold_sum(rows, axis):
    size = lax.axis_size(axis)
    fold = fold_of(axis)
    groups = size // fold
    rank = lax.axis_index(axis)
    blocks = rows.reshape((groups, fold, rows.shape[0] // size) + rows.shape[1:])
    mine = rank % fold
    half = lax.dynamic_index_in_dim(blocks, mine, 1, False)
    if fold > 1:
        arrived = lax.ppermute(
            lax.dynamic_index_in_dim(blocks, 1 - mine, 1, False),
            axis,
            [(i, i ^ 1) for i in range(size)],
        )
        half = (half.astype(jnp.float32) + arrived.astype(jnp.float32)).astype(rows.dtype)
    group = rank // fold
    total = lax.dynamic_index_in_dim(half, group, 0, False).astype(jnp.float32)
    for step in range(1, groups):
        block = lax.dynamic_index_in_dim(half, (group + step) % groups, 0, False)
        arrived = shifted(block, axis, step * fold)
        total = total + arrived.astype(jnp.float32)
    return total


def fold_gather(rows, axis):
    size = lax.axis_size(axis)
    fold = fold_of(axis)
    groups = size // fold
    rank = lax.axis_index(axis)
    group = rank // fold
    held = jnp.zeros((groups,) + rows.shape, rows.dtype)
    held = lax.dynamic_update_index_in_dim(held, rows, group, 0)
    for step in range(1, groups):
        arrived = shifted(rows, axis, step * fold)
        held = lax.dynamic_update_index_in_dim(
            held, arrived, (group + groups - step) % groups, 0
        )
    if fold == 1:
        return held.reshape((size * rows.shape[0],) + rows.shape[1:])
    other = lax.ppermute(held, axis, [(i, i ^ 1) for i in range(size)])
    even = rank % 2 == 0
    both = jnp.stack([jnp.where(even, held, other), jnp.where(even, other, held)], axis=1)
    return both.reshape((size * rows.shape[0],) + rows.shape[1:])


def scatter_columns(part, axis):
    size = lax.axis_size(axis)
    rank = lax.axis_index(axis)
    width = part.shape[1] // size
    arrived = [
        lax.ppermute(
            lax.dynamic_slice_in_dim(part, ((rank + step) % size) * width, width, 1),
            axis,
            [(i, (i + step) % size) for i in range(size)],
        )
        for step in range(1, size)
    ]
    total = lax.dynamic_slice_in_dim(part, rank * width, width, 1).astype(jnp.float32)
    for block in arrived:
        total = total + block.astype(jnp.float32)
    return total


def write_kernel(starts, key_in, value_in, key_new, value_new, key_out, value_out):
    seqs, span = key_in.shape[:2]
    members = key_new.shape[1]
    key_out[...] = key_in[...]
    value_out[...] = value_in[...]
    for local in range(seqs):
        start = starts[pl.program_id(0) * seqs + local]

        @pl.when((start > -members) & (start < span))
        def _():
            def place(member, carry):
                spot = start + member

                @pl.when((spot >= 0) & (spot < span))
                def _():
                    key_out[local, spot] = key_new[local, member]
                    value_out[local, spot] = value_new[local, member]

                return carry

            lax.fori_loop(0, members, place, 0)


def write_rows(starts, key_cache, value_cache, key_new, value_new):
    num_seqs, span, heads, width = key_cache.shape
    members = key_new.shape[1]
    step = 2 if num_seqs % 2 == 0 else 1
    cache_spec = pl.BlockSpec((step, span, heads, width), lambda s, starts: (s, 0, 0, 0))
    new_spec = pl.BlockSpec((step, members, heads, width), lambda s, starts: (s, 0, 0, 0))
    shape = jax.ShapeDtypeStruct(key_cache.shape, key_cache.dtype)
    return pl.pallas_call(
        write_kernel,
        out_shape=(shape, shape),
        grid_spec=pltpu.PrefetchScalarGridSpec(
            num_scalar_prefetch=1,
            grid=(num_seqs // step,),
            in_specs=[cache_spec, cache_spec, new_spec, new_spec],
            out_specs=(cache_spec, cache_spec),
        ),
        cost_estimate=pl.CostEstimate(
            flops=8 * key_cache.size, bytes_accessed=8 * key_cache.size, transcendentals=0
        ),
    )(starts, key_cache, value_cache, key_new, value_new)


def ancestry(parent_ids, members):
    identity = jnp.eye(members, dtype=jnp.float32)
    parent_hot = (
        parent_ids[:, :, None] == jnp.arange(members, dtype=jnp.int32)[None, None, :]
    ).astype(jnp.float32)
    ancestors = jnp.minimum(identity[None] + parent_hot, 1.0)
    for _ in range(max(1, (members - 1).bit_length())):
        ancestors = jnp.minimum(
            jnp.einsum("bij,bjk->bik", ancestors, ancestors, precision=lax.Precision.HIGHEST), 1.0
        )
    return ancestors


def finish_rows(cache_max, cache_total, cache_values, last_rows, tree_max, tree_total, tree_values):
    shifted = cache_max + last_rows
    top = jnp.maximum(shifted, tree_max)
    cache_scale = jnp.exp(shifted - top)
    tree_scale = jnp.exp(tree_max - top)
    attended = (
        (cache_values * cache_scale[..., None] + tree_values * tree_scale[..., None])
        / (cache_total * cache_scale + tree_total * tree_scale)[..., None]
    ).astype(jnp.bfloat16)
    return attended.reshape(attended.shape[0], attended.shape[1] * attended.shape[2])


def per_device(
    tokens,
    gain_pre,
    w_query,
    w_key,
    w_value,
    w_forget,
    b_forget,
    w_out,
    gain_post,
    key_cache,
    value_cache,
    cum_cache,
    lengths,
    accepted,
    parent,
):
    num_seqs, proposals, model_width = tokens.shape
    kv_rank = lax.axis_index("kv")
    tp_rank = lax.axis_index("tp")
    span = key_cache.shape[1]
    heads_local = key_cache.shape[2]
    head_dim = key_cache.shape[3]
    scale = head_dim ** (-0.5)
    all_rows = num_seqs * proposals
    weight_rows = w_query.shape[0]
    tok_float = tokens.astype(jnp.float32)
    inverse = lax.rsqrt(jnp.mean(tok_float * tok_float, -1, keepdims=True) + epsilon)
    local_first = kv_rank * weight_rows
    local_rows = (
        (
            lax.dynamic_slice_in_dim(tokens, local_first, weight_rows, 2).astype(jnp.float32)
            * inverse
            * lax.dynamic_slice_in_dim(gain_pre, local_first, weight_rows, 0)
        )
        .astype(jnp.bfloat16)
        .reshape(all_rows, weight_rows)
    )
    query_part = jnp.dot(local_rows, w_query, preferred_element_type=jnp.float32)
    kv_size = lax.axis_size("kv")
    rows_local = all_rows // kv_size
    query_in = exchange(query_part.astype(jnp.bfloat16), "kv")
    own_queries = jnp.sum(query_in.astype(jnp.float32), axis=0).astype(jnp.bfloat16)
    query_all = gather_rows(own_queries, "kv")
    flat = (tok_float * inverse * gain_pre).astype(jnp.bfloat16).reshape(all_rows, model_width)
    key_part = jnp.dot(local_rows, w_key, preferred_element_type=jnp.float32)
    value_part = jnp.dot(local_rows, w_value, preferred_element_type=jnp.float32)
    forget_cols = lax.dynamic_slice_in_dim(w_forget, tp_rank * heads_local, heads_local, 1)
    forget_bias = lax.dynamic_slice_in_dim(b_forget, tp_rank * heads_local, heads_local, 0)
    log_forget = jax.nn.log_sigmoid(
        jnp.dot(flat, forget_cols, preferred_element_type=jnp.float32) + forget_bias
    ).reshape(num_seqs, proposals, heads_local)
    ancestors = ancestry(parent, proposals)
    path = jnp.einsum("bij,bjh->bih", ancestors, log_forget, precision=lax.Precision.HIGHEST)
    valid = lengths + accepted
    positions = kv_rank * span + jnp.arange(span, dtype=jnp.int32)
    owner = positions[None, :] == (valid - 1)[:, None]
    last_part = jnp.sum(jnp.where(owner[:, :, None], cum_cache, 0.0), axis=1)
    last_part = jnp.broadcast_to(
        last_part[:, None, :], (num_seqs, proposals, heads_local)
    ).reshape(all_rows, heads_local)
    own_row = kv_rank * rows_local
    seqs_local = max(1, rows_local // proposals)
    own_seq = own_row // proposals
    rows_each = rows_local // seqs_local
    head_width = heads_local * head_dim
    lanes = -(-3 * heads_local // 128) * 128
    sent = jnp.concatenate(
        [
            key_part.astype(jnp.bfloat16),
            value_part.astype(jnp.bfloat16),
            pack_lanes(last_part, lanes),
        ],
        axis=1,
    )
    own = fold_sum(sent, "kv").astype(jnp.bfloat16)
    full = fold_gather(own, "kv")
    own_last = unpack_lanes(own[:, 2 * head_width :], heads_local)
    last_rows_all = unpack_lanes(full[:, 2 * head_width :], heads_local)
    last_cum = last_rows_all.reshape(num_seqs, proposals, heads_local)[:, 0]
    query = query_all.reshape(num_seqs, proposals, heads_local, head_dim)
    key_new = full[:, :head_width].reshape(num_seqs, proposals, heads_local, head_dim)
    value_new = full[:, head_width : 2 * head_width].reshape(
        num_seqs, proposals, heads_local, head_dim
    )
    live = (positions[None, :] < valid[:, None])[:, None, None, :]
    score = (
        jnp.einsum("bihd,bkhd->bihk", query, key_cache, preferred_element_type=jnp.float32) * scale
        + path[..., None]
        - jnp.swapaxes(cum_cache, 1, 2)[:, None]
    )
    block_max = jnp.max(jnp.where(live, score, floor_value), axis=-1)
    weight = jnp.exp(jnp.where(live, score - block_max[..., None], floor_value))
    block_total = jnp.sum(weight, axis=-1)
    block_values = jnp.einsum(
        "bihk,bkhd->bihd",
        weight.astype(jnp.bfloat16),
        value_cache,
        preferred_element_type=jnp.float32,
    )
    has_live = block_total > 0.0
    safe_total = jnp.where(has_live, block_total, 1.0)
    block_mean = (block_values / safe_total[..., None]).astype(jnp.bfloat16)
    block_log = jnp.where(has_live, block_max + jnp.log(safe_total), floor_value)
    blocks_in = exchange(
        jnp.concatenate(
            [
                block_mean.reshape(all_rows, head_width),
                pack_lanes(block_log.reshape(all_rows, heads_local), lanes),
            ],
            axis=1,
        ),
        "kv",
    )
    own_query = own_queries.reshape(seqs_local, rows_each, heads_local, head_dim)
    if rows_local % proposals == 0:
        pair = own[:, : 2 * head_width].reshape(seqs_local, proposals, 2, heads_local, head_dim)
        own_keys = pair[:, :, 0]
        own_values = pair[:, :, 1]
    else:
        own_keys = lax.dynamic_slice_in_dim(key_new, own_seq, seqs_local, 0)
        own_values = lax.dynamic_slice_in_dim(value_new, own_seq, seqs_local, 0)
    seq_path = lax.dynamic_slice_in_dim(path, own_seq, seqs_local, 0)
    own_path = lax.dynamic_slice_in_dim(
        path.reshape(all_rows, heads_local), own_row, rows_local, 0
    ).reshape(seqs_local, rows_each, heads_local)
    own_ancestors = lax.dynamic_slice_in_dim(
        ancestors.reshape(all_rows, proposals), own_row, rows_local, 0
    ).reshape(seqs_local, rows_each, proposals)
    tree_mask = (own_ancestors > 0.5)[:, :, None, :]
    tree_score = (
        jnp.einsum("bihd,bjhd->bihj", own_query, own_keys, preferred_element_type=jnp.float32)
        * scale
        + own_path[..., None]
        - jnp.swapaxes(seq_path, 1, 2)[:, None]
    )
    tree_max = jnp.max(jnp.where(tree_mask, tree_score, floor_value), axis=-1)
    tree_weight = jnp.exp(jnp.where(tree_mask, tree_score - tree_max[..., None], floor_value))
    tree_total = jnp.sum(tree_weight, axis=-1)
    tree_values = jnp.einsum(
        "bihj,bjhd->bihd",
        tree_weight.astype(jnp.bfloat16),
        own_values,
        preferred_element_type=jnp.float32,
    )
    logs_in = unpack_lanes(blocks_in[:, :, head_width:], heads_local)
    cache_max = jnp.max(logs_in, axis=0)
    shares = jnp.exp(logs_in - cache_max[None])
    cache_total = jnp.sum(shares, axis=0)
    cache_values = jnp.sum(
        blocks_in[:, :, :head_width]
        .astype(jnp.float32)
        .reshape(kv_size, rows_local, heads_local, head_dim)
        * shares[..., None],
        axis=0,
    )
    own_attended = finish_rows(
        cache_max,
        cache_total,
        cache_values,
        own_last,
        tree_max.reshape(rows_local, heads_local),
        tree_total.reshape(rows_local, heads_local),
        tree_values.reshape(rows_local, heads_local, head_dim),
    )
    attended = gather_rows(own_attended, "kv")
    mixed_part = jnp.dot(attended, w_out, preferred_element_type=jnp.float32)
    mixed_sum = scatter_columns(mixed_part.astype(jnp.bfloat16), "tp")
    own_squares = jnp.sum(mixed_sum * mixed_sum, axis=1)
    squares = jnp.sum(
        gather_rows(own_squares[None], ("kv", "tp")), axis=0
    )
    mixed = (mixed_sum * lax.rsqrt(squares / model_width + epsilon)[:, None] * gain_post).astype(
        jnp.bfloat16
    )
    mixed = mixed.reshape(num_seqs, proposals, mixed_sum.shape[1])
    relative = positions[None, :] - valid[:, None]
    select = relative[:, :, None] == jnp.arange(proposals, dtype=jnp.int32)[None, None, :]
    written = (relative >= 0) & (relative < proposals)
    key_out, value_out = write_rows(
        valid - kv_rank * span, key_cache, value_cache, key_new, value_new
    )
    cum_new = last_cum[:, None, :] + path
    placed_cum = jnp.einsum(
        "bkj,bjh->bkh", select.astype(jnp.float32), cum_new, precision=lax.Precision.HIGHEST
    )
    cum_out = jnp.where(written[:, :, None], placed_cum, cum_cache)
    return (mixed, key_out, value_out, cum_out)


def solution(mesh):
    return jax.shard_map(
        per_device,
        mesh=mesh,
        in_specs=(
            P(),
            P(),
            P("kv", "tp"),
            P("kv", "tp"),
            P("kv", "tp"),
            P(),
            P(),
            P("tp", "kv"),
            P(("kv", "tp")),
            P(None, "kv", "tp", None),
            P(None, "kv", "tp", None),
            P(None, "kv", "tp"),
            P(),
            P(),
            P(),
        ),
        out_specs=(
            P(None, None, ("kv", "tp")),
            P(None, "kv", "tp", None),
            P(None, "kv", "tp", None),
            P(None, "kv", "tp"),
        ),
        check_vma=False,
    )
```

profile of v0, /device:TPU:0, one launch (start us, length us, event | category | flops | bytes accessed | tf_op | source)
XLA Modules:
  0.0 163.9 jit_solution(13967284593922334621)
XLA Ops:
  0.7 2.2 %fusion = f32[16,16]{1,0:T(8,128)S(1)} fusion(bf16[16,16,4096]{2,1,0:T(8,128)(2,1)} %param.15), kind=kLoop, calls=%fused_computation.2 | loop fusion | flops 3145472 | bytes 2098176 | tf_op jit(solution)/shard_map/reduce_sum | solution.py:215
  4.2 7.3 %all-to-all-start = ((bf16[8,32,512]{2,1,0:T(8,128)(2,1)}), bf16[8,32,512]{2,1,0:T(8,128)(2,1)S(1)}, u32[]{:S(2)}, u32[]{:S(2)}) async-start(bf16[8,32,512]{2,1,0:T(8,128)(2,1)} %bitcast.1), calls=%async_computation | async-start | bytes 524288 | tf_op jit(solution)/shard_map/all_to_all | solution.py:43
  13.3 1.3 convolution_convert_fusion.1
  14.6 2.0 %convolution_convert_fusion.2 = bf16[256,512]{1,0:T(8,128)(2,1)} fusion(bf16[256,512]{1,0:T(8,128)(2,1)S(1)} %bitcast.123, bf16[512,512]{1,0:T(8,128)(2,1)} %param.18), kind=kOutput, calls=%fused_computation.19 | convolution fusion | flops 134348800 | bytes 1048576 | tf_op jit(solution)/shard_map/dot_general | solution.py:233
  18.4 2.0 %collective-permute-start = (bf16[4,32,1152]{2,1,0:T(8,128)(2,1)}, bf16[4,32,1152]{2,1,0:T(8,128)(2,1)}, u32[]{:S(2)}, u32[]{:S(2)}) collective-permute-start(bf16[4,32,1152]{2,1,0:T(8,128)(2,1)} %get-tuple-element.23), channel_id=1, source_target_pairs={{0,4},{4,0},{8,12},{12,8},{16,20},{20,16},{24,28},{28,24},{1,5},{5... | collective-permute-start | bytes 884744 | tf_op jit(solution)/shard_map/ppermute | solution.py:64
  20.4 1.9 %fusion.2 = bf16[16,16,4096]{2,1,0:T(8,128)(2,1)} fusion(bf16[16,16,4096]{2,1,0:T(8,128)(2,1)S(1)} %copy-done.1, f32[4096]{0:T(1024)S(1)} %copy-done.11, f32[16,16]{1,0:T(8,128)S(1)} %add_rsqrt_fusion), kind=kLoop, calls=%fused_computation.4 | loop fusion | flops 4194304 | bytes 4211712 | tf_op jit(solution)/shard_map/convert_element_type | solution.py:232
  23.6 1.4 copy.282
  25.1 1.5 fusion.73
  28.6 1.5 copy.253
  30.5 1.5 collective-permute-start.1
  32.0 2.4 %collective-permute-start.3 = (bf16[32,1152]{0,1:T(8,128)(2,1)S(1)}, bf16[32,1152]{0,1:T(8,128)(2,1)S(1)}, u32[]{:S(2)}, u32[]{:S(2)}) collective-permute-start(bf16[32,1152]{0,1:T(8,128)(2,1)S(1)} %get-tuple-element.16), channel_id=1, source_target_pairs={{0,24},{4,28},{8,0},{12,4},{16,8},{20,12},{24,16},{28,20},{1,25},{... | collective-permute-start | bytes 221192 | tf_op jit(solution)/shard_map/ppermute | solution.py:48
  35.5 6.7 %collective-permute-done.1 = bf16[32,1152]{0,1:T(8,128)(2,1)S(1)} collective-permute-done((bf16[32,1152]{0,1:T(8,128)(2,1)S(1)}, bf16[32,1152]{0,1:T(8,128)(2,1)S(1)}, u32[]{:S(2)}, u32[]{:S(2)}) %collective-permute-start.1) | collective-permute-done | bytes 73760 | tf_op jit(solution)/shard_map/ppermute | solution.py:48
  42.2 3.7 %collective-permute-done.3 = bf16[32,1152]{0,1:T(8,128)(2,1)S(1)} collective-permute-done((bf16[32,1152]{0,1:T(8,128)(2,1)S(1)}, bf16[32,1152]{0,1:T(8,128)(2,1)S(1)}, u32[]{:S(2)}, u32[]{:S(2)}) %collective-permute-start.3) | collective-permute-done | bytes 73760 | tf_op jit(solution)/shard_map/ppermute | solution.py:48
  45.9 13.3 %collective-permute-done.2 = bf16[32,1152]{0,1:T(8,128)(2,1)S(1)} collective-permute-done((bf16[32,1152]{0,1:T(8,128)(2,1)S(1)}, bf16[32,1152]{0,1:T(8,128)(2,1)S(1)}, u32[]{:S(2)}, u32[]{:S(2)}) %collective-permute-start.2) | collective-permute-done | bytes 73760 | tf_op jit(solution)/shard_map/ppermute | solution.py:48
  60.0 1.5 collective-permute-start.9
  63.2 1.6 fusion.87
  64.8 16.1 %collective-permute-done.7 = bf16[32,1152]{0,1:T(8,128)(2,1)} collective-permute-done((bf16[32,1152]{0,1:T(8,128)(2,1)S(1)}, bf16[32,1152]{0,1:T(8,128)(2,1)}, u32[]{:S(2)}, u32[]{:S(2)}) %collective-permute-start.7) | collective-permute-done | bytes 73760 | tf_op jit(solution)/shard_map/ppermute | solution.py:48
  83.1 2.8 %collective-permute-done.8 = bf16[32,1152]{0,1:T(8,128)(2,1)} collective-permute-done((bf16[32,1152]{0,1:T(8,128)(2,1)S(1)}, bf16[32,1152]{0,1:T(8,128)(2,1)}, u32[]{:S(2)}, u32[]{:S(2)}) %collective-permute-start.8) | collective-permute-done | bytes 73760 | tf_op jit(solution)/shard_map/ppermute | solution.py:48
  88.2 8.1 %all-to-all-start.1 = ((bf16[8,32,512]{2,1,0:T(8,128)(2,1)}), bf16[8,32,512]{2,1,0:T(8,128)(2,1)S(1)}, u32[]{:S(2)}, u32[]{:S(2)}) async-start(bf16[8,32,512]{2,1,0:T(8,128)(2,1)} %broadcast_in_dim.132), calls=%async_computation.1 | async-start | bytes 524288 | tf_op jit(solution)/shard_map/all_to_all | solution.py:35
  99.1 6.1 %all-to-all-done.1 = bf16[8,32,512]{2,1,0:T(8,128)(2,1)S(1)} async-done(((bf16[8,32,512]{2,1,0:T(8,128)(2,1)}), bf16[8,32,512]{2,1,0:T(8,128)(2,1)S(1)}, u32[]{:S(2)}, u32[]{:S(2)}) %all-to-all-start.1) | async-done | bytes 262176 | tf_op jit(solution)/shard_map/all_to_all | solution.py:35
  105.3 2.8 %select_reduce_fusion = (f32[16,16,4]{1,2,0:T(4,128)S(1)}, f32[16,16,4,128]{3,1,2,0:T(8,128)}) fusion(pred[16,128]{1,0:T(8,128)(4,1)S(1)} %get-tuple-element.36, f32[16,4,128]{2,1,0:T(4,128)} %bitcast.137, f32[16,16,4]{1,2,0:T(4,128)S(1)} %copy-done.7, bf16[16,128,4,128]{3,2,1,0:T(4,128)(2,1)S(1)} %copy-done.4, bf16[16,16,4,128]{3,2,1,0:T(4,128)(2,1)S(1)} %reshape_reshape.3), kind=kOutput, calls=%fused_computation.44 | convolution fusion | flops 34208768 | bytes 2926592 | tf_op jit(solution)/shard_map/bihd,bkhd->bihk/dot_general | solution.py:275
  108.0 1.4 fusion.38
  109.7 2.5 %fusion.26 = bf16[16,16,4,128]{3,1,2,0:T(8,128)(2,1)S(1)} fusion(bf16[16,128,4,128]{3,2,1,0:T(4,128)(2,1)} %value_in.1, f32[16,16,4,128]{3,1,2,0:T(8,128)} %get-tuple-element.41, f32[16,16,4]{1,2,0:T(4,128)S(1)} %compare_select_fusion, f32[16,16,4]{1,2,0:T(4,128)S(1)} %get-tuple-element.40, pred[16,128]{1,0:T(8,128)(4,1)S(1)} %get-tuple-element.36), kind=kOutput, calls=%fused_computation.21 | convolution fusion | flops 34209792 | bytes 2893824 | tf_op jit(solution)/shard_map/bihk,bkhd->bihd/dot_general | solution.py:282
  113.4 3.6 %all-to-all-start.2 = ((bf16[8,32,640]{2,1,0:T(8,128)(2,1)}), bf16[8,32,640]{2,1,0:T(8,128)(2,1)S(1)}, u32[]{:S(2)}, u32[]{:S(2)}) async-start(bf16[8,32,640]{2,1,0:T(8,128)(2,1)} %pad_maximum_fusion.1), calls=%async_computation.2 | async-start | bytes 655360 | tf_op jit(solution)/shard_map/all_to_all | solution.py:43
  118.1 8.8 %all-to-all-done.2 = bf16[8,32,640]{2,1,0:T(8,128)(2,1)S(1)} async-done(((bf16[8,32,640]{2,1,0:T(8,128)(2,1)}), bf16[8,32,640]{2,1,0:T(8,128)(2,1)S(1)}, u32[]{:S(2)}, u32[]{:S(2)}) %all-to-all-start.2) | async-done | bytes 327712 | tf_op jit(solution)/shard_map/all_to_all | solution.py:43
  130.2 3.7 %all-to-all-start.3 = ((bf16[8,32,512]{2,1,0:T(8,128)(2,1)}), bf16[8,32,512]{2,1,0:T(8,128)(2,1)S(1)}, u32[]{:S(2)}, u32[]{:S(2)}) async-start(bf16[8,32,512]{2,1,0:T(8,128)(2,1)} %broadcast_in_dim.142), calls=%async_computation.3 | async-start | bytes 524288 | tf_op jit(solution)/shard_map/all_to_all | solution.py:35
  134.0 8.5 %all-to-all-done.3 = bf16[8,32,512]{2,1,0:T(8,128)(2,1)S(1)} async-done(((bf16[8,32,512]{2,1,0:T(8,128)(2,1)}), bf16[8,32,512]{2,1,0:T(8,128)(2,1)S(1)}, u32[]{:S(2)}, u32[]{:S(2)}) %all-to-all-start.3) | async-done | bytes 262176 | tf_op jit(solution)/shard_map/all_to_all | solution.py:35
  142.9 1.7 %collective-permute-start.6 = (bf16[256,128]{1,0:T(8,128)(2,1)S(1)}, bf16[256,128]{1,0:T(8,128)(2,1)S(1)}, u32[]{:S(2)}, u32[]{:S(2)}) collective-permute-start(bf16[256,128]{1,0:T(8,128)(2,1)S(1)} %get-tuple-element.25), channel_id=1, source_target_pairs={{0,3},{1,0},{2,1},{3,2},{4,7},{5,4},{6,5},{7,6},{8,11},{9,8},{10,9... | collective-permute-start | bytes 196616 | tf_op jit(solution)/shard_map/ppermute | solution.py:105
  144.6 1.5 collective-permute-start.5
  147.0 2.2 %collective-permute-done.5 = bf16[256,128]{1,0:T(8,128)(2,1)S(1)} collective-permute-done((bf16[256,128]{1,0:T(8,128)(2,1)S(1)}, bf16[256,128]{1,0:T(8,128)(2,1)S(1)}, u32[]{:S(2)}, u32[]{:S(2)}) %collective-permute-start.5) | collective-permute-done | bytes 65568 | tf_op jit(solution)/shard_map/ppermute | solution.py:105
  149.9 3.3 %all-to-all-start.4 = ((f32[32,1,256]{2,1,0:T(1,128)}), f32[32,1,256]{2,1,0:T(1,128)S(1)}, u32[]{:S(2)}, u32[]{:S(2)}) async-start(f32[32,1,256]{2,1,0:T(1,128)} %broadcast_in_dim.143), calls=%async_computation.4 | async-start | bytes 65536 | tf_op jit(solution)/shard_map/all_to_all | solution.py:35
  155.6 7.4 %shard_map.174 = (bf16[16,128,4,128]{3,2,1,0:T(4,128)(2,1)}, bf16[16,128,4,128]{3,2,1,0:T(4,128)(2,1)}) custom-call(s32[16]{0:T(128)} %get-tuple-element.8.starts, bf16[16,128,4,128]{3,2,1,0:T(4,128)(2,1)} %key_in.1, bf16[16,128,4,128]{3,2,1,0:T(4,128)(2,1)} %value_in.1, bf16[16,16,4,128]{3,2,1,0:T(4,128)(2,1)} %reshape.290.key_new, ...), custom_call_target="tpu_custom_call" | custom-call | flops 8388608 | bytes 8388608 | tf_op jit(solution)/shard_map/pallas_call | solution.py:148
  (160 shorter events, 30.2 us)
Async XLA Ops:
  0.7 10.8 %copy-start.16 = (s32[16]{0:T(128)S(1)}, s32[16]{0:T(128)}, u32[]{:S(2)}) copy-start(s32[16]{0:T(128)} %param.27) | copy-start | bytes 196
  0.7 10.8 %copy-start.17 = (s32[16]{0:T(128)S(1)}, s32[16]{0:T(128)}, u32[]{:S(2)}) copy-start(s32[16]{0:T(128)} %param.28) | copy-start | bytes 196
  0.7 12.1 %copy-start.9 = (f32[16,128,4]{1,2,0:T(4,128)S(1)}, f32[16,128,4]{1,2,0:T(4,128)}, u32[]{:S(2)}) copy-start(f32[16,128,4]{1,2,0:T(4,128)} %param.26) | copy-start | bytes 98308
  4.2 83.2 %all-to-all-start = ((bf16[8,32,512]{2,1,0:T(8,128)(2,1)}), bf16[8,32,512]{2,1,0:T(8,128)(2,1)S(1)}, u32[]{:S(2)}, u32[]{:S(2)}) async-start(bf16[8,32,512]{2,1,0:T(8,128)(2,1)} %bitcast.1), calls=%async_computation | async-start | bytes 524288 | tf_op jit(solution)/shard_map/all_to_all | solution.py:43
  18.4 10.2 %collective-permute-start = (bf16[4,32,1152]{2,1,0:T(8,128)(2,1)}, bf16[4,32,1152]{2,1,0:T(8,128)(2,1)}, u32[]{:S(2)}, u32[]{:S(2)}) collective-permute-start(bf16[4,32,1152]{2,1,0:T(8,128)(2,1)} %get-tuple-element.23), channel_id=1, source_target_pairs={{0,4},{4,0},{8,12},{12,8},{16,20},{20,16},{24,28},{28,24},{1,5},{5... | collective-permute-start | bytes 884744 | tf_op jit(solution)/shard_map/ppermute | solution.py:64
  22.4 2.7 %copy-start.19 = (f32[16]{0:T(128)S(1)}, f32[16]{0:T(128)}, u32[]{:S(2)}) copy-start(f32[16]{0:T(128)} %param.21) | copy-start | bytes 196
  22.4 2.7 %copy-start.2 = (bf16[16,16,4096]{2,1,0:T(8,128)(2,1)S(1)}, bf16[16,16,4096]{2,1,0:T(8,128)(2,1)}, u32[]{:S(2)}) copy-start(bf16[16,16,4096]{2,1,0:T(8,128)(2,1)} %fusion.2) | copy-start | bytes 6291460
  26.6 3.5 %copy-start.3 = (bf16[4,1,32,1152]{2,3,0,1:T(8,128)(2,1)S(1)}, bf16[4,1,32,1152]{2,3,0,1:T(8,128)(2,1)}, u32[]{:S(2)}) copy-start(bf16[4,1,32,1152]{2,3,0,1:T(8,128)(2,1)} %copy.282) | copy-start | bytes 884740
  27.1 7.9 %copy-start.6 = (f32[16,16,4]{1,2,0:T(4,128)}, f32[16,16,4]{1,2,0:T(4,128)S(1)}, u32[]{:S(2)}) copy-start(f32[16,16,4]{1,2,0:T(4,128)S(1)} %fusion.58) | copy-start | bytes 12292
  30.5 11.8 %collective-permute-start.1 = (bf16[32,1152]{0,1:T(8,128)(2,1)S(1)}, bf16[32,1152]{0,1:T(8,128)(2,1)S(1)}, u32[]{:S(2)}, u32[]{:S(2)}) collective-permute-start(bf16[32,1152]{0,1:T(8,128)(2,1)S(1)} %get-tuple-element.15), channel_id=1, source_target_pairs={{0,8},{4,12},{8,16},{12,20},{16,24},{20,28},{24,0},{28,4},{1,9},{5... | collective-permute-start | bytes 221192 | tf_op jit(solution)/shard_map/ppermute | solution.py:48
  32.0 13.9 %collective-permute-start.3 = (bf16[32,1152]{0,1:T(8,128)(2,1)S(1)}, bf16[32,1152]{0,1:T(8,128)(2,1)S(1)}, u32[]{:S(2)}, u32[]{:S(2)}) collective-permute-start(bf16[32,1152]{0,1:T(8,128)(2,1)S(1)} %get-tuple-element.16), channel_id=1, source_target_pairs={{0,24},{4,28},{8,0},{12,4},{16,8},{20,12},{24,16},{28,20},{1,25},{... | collective-permute-start | bytes 221192 | tf_op jit(solution)/shard_map/ppermute | solution.py:48
  34.4 24.8 %collective-permute-start.2 = (bf16[32,1152]{0,1:T(8,128)(2,1)S(1)}, bf16[32,1152]{0,1:T(8,128)(2,1)S(1)}, u32[]{:S(2)}, u32[]{:S(2)}) collective-permute-start(bf16[32,1152]{0,1:T(8,128)(2,1)S(1)} %get-tuple-element.17), channel_id=1, source_target_pairs={{0,16},{4,20},{8,24},{12,28},{16,0},{20,4},{24,8},{28,12},{1,17},{... | collective-permute-start | bytes 221192 | tf_op jit(solution)/shard_map/ppermute | solution.py:48
  60.0 22.0 %collective-permute-start.9 = (bf16[32,1152]{0,1:T(8,128)(2,1)S(1)}, bf16[32,1152]{0,1:T(8,128)(2,1)}, u32[]{:S(2)}, u32[]{:S(2)}) collective-permute-start(bf16[32,1152]{0,1:T(8,128)(2,1)S(1)} %fusion.37), channel_id=1, source_target_pairs={{0,24},{4,28},{8,0},{12,4},{16,8},{20,12},{24,16},{28,20},{1,25},{... | collective-permute-start | bytes 221192 | tf_op jit(solution)/shard_map/ppermute | solution.py:48
  61.6 24.3 %collective-permute-start.8 = (bf16[32,1152]{0,1:T(8,128)(2,1)S(1)}, bf16[32,1152]{0,1:T(8,128)(2,1)}, u32[]{:S(2)}, u32[]{:S(2)}) collective-permute-start(bf16[32,1152]{0,1:T(8,128)(2,1)S(1)} %fusion.37), channel_id=1, source_target_pairs={{0,16},{4,20},{8,24},{12,28},{16,0},{20,4},{24,8},{28,12},{1,17},{... | collective-permute-start | bytes 221192 | tf_op jit(solution)/shard_map/ppermute | solution.py:48
  61.6 19.3 %collective-permute-start.7 = (bf16[32,1152]{0,1:T(8,128)(2,1)S(1)}, bf16[32,1152]{0,1:T(8,128)(2,1)}, u32[]{:S(2)}, u32[]{:S(2)}) collective-permute-start(bf16[32,1152]{0,1:T(8,128)(2,1)S(1)} %fusion.37), channel_id=1, source_target_pairs={{0,8},{4,12},{8,16},{12,20},{16,24},{20,28},{24,0},{28,4},{1,9},{5... | collective-permute-start | bytes 221192 | tf_op jit(solution)/shard_map/ppermute | solution.py:48
  63.2 42.1 %copy-start.4 = (bf16[16,128,4,128]{3,2,1,0:T(4,128)(2,1)S(1)}, bf16[16,128,4,128]{3,2,1,0:T(4,128)(2,1)}, u32[]{:S(2)}) copy-start(bf16[16,128,4,128]{3,2,1,0:T(4,128)(2,1)} %key_in.1) | copy-start | bytes 6291460
  85.9 19.4 %copy-start.7 = (f32[16,16,4]{1,2,0:T(4,128)S(1)}, f32[16,16,4]{1,2,0:T(4,128)}, u32[]{:S(2)}) copy-start(f32[16,16,4]{1,2,0:T(4,128)} %copy-done.6) | copy-start | bytes 12292
  87.1 29.9 %collective-permute-start.10 = (bf16[4,32,1152]{2,1,0:T(8,128)(2,1)S(1)}, bf16[4,32,1152]{2,1,0:T(8,128)(2,1)}, u32[]{:S(2)}, u32[]{:S(2)}) collective-permute-start(bf16[4,32,1152]{2,1,0:T(8,128)(2,1)S(1)} %constant_dynamic-update-slice_fusion), channel_id=1, source_target_pairs={{0,4},{4,0},{8,12},{12,8},{16,20},{20,16},{24,28},{28,24},{1,5},{5... | collective-permute-start | bytes 884744 | tf_op jit(solution)/shard_map/ppermute | solution.py:94
  88.2 17.0 %all-to-all-start.1 = ((bf16[8,32,512]{2,1,0:T(8,128)(2,1)}), bf16[8,32,512]{2,1,0:T(8,128)(2,1)S(1)}, u32[]{:S(2)}, u32[]{:S(2)}) async-start(bf16[8,32,512]{2,1,0:T(8,128)(2,1)} %broadcast_in_dim.132), calls=%async_computation.1 | async-start | bytes 524288 | tf_op jit(solution)/shard_map/all_to_all | solution.py:35
  113.4 13.6 %all-to-all-start.2 = ((bf16[8,32,640]{2,1,0:T(8,128)(2,1)}), bf16[8,32,640]{2,1,0:T(8,128)(2,1)S(1)}, u32[]{:S(2)}, u32[]{:S(2)}) async-start(bf16[8,32,640]{2,1,0:T(8,128)(2,1)} %pad_maximum_fusion.1), calls=%async_computation.2 | async-start | bytes 655360 | tf_op jit(solution)/shard_map/all_to_all | solution.py:43
  117.0 10.4 %copy-start.12 = (f32[32,4]{0,1:T(4,128)S(1)}, f32[32,4]{0,1:T(4,128)}, u32[]{:S(2)}) copy-start(f32[32,4]{0,1:T(4,128)} %reshape.284) | copy-start | bytes 1540
  128.8 13.7 %copy-start.5 = (bf16[512,512]{1,0:T(8,128)(2,1)S(1)}, bf16[512,512]{1,0:T(8,128)(2,1)}, u32[]{:S(2)}) copy-start(bf16[512,512]{1,0:T(8,128)(2,1)} %param.22) | copy-start | bytes 1572868
  130.2 23.0 %copy-start.8 = (f32[16,16,4]{1,2,0:T(4,128)S(1)}, f32[16,16,4]{1,2,0:T(4,128)}, u32[]{:S(2)}) copy-start(f32[16,16,4]{1,2,0:T(4,128)} %copy-done.6) | copy-start | bytes 12292
  130.2 23.0 %copy-start.10 = (f32[16,128,4]{1,2,0:T(4,128)S(1)}, f32[16,128,4]{1,2,0:T(4,128)}, u32[]{:S(2)}) copy-start(f32[16,128,4]{1,2,0:T(4,128)} %param.26) | copy-start | bytes 98308
  130.2 23.0 %copy-start.13 = (s32[16,128]{1,0:T(8,128)S(1)}, s32[16,128]{1,0:T(8,128)}, u32[]{:S(2)}) copy-start(s32[16,128]{1,0:T(8,128)} %broadcast_subtract_fusion) | copy-start | bytes 24580
  130.2 23.1 %copy-start.14 = (pred[16,128]{1,0:T(8,128)(4,1)S(1)}, pred[16,128]{1,0:T(8,128)(4,1)}, u32[]{:S(2)}) copy-start(pred[16,128]{1,0:T(8,128)(4,1)} %get-tuple-element.35) | copy-start | bytes 6148
  130.2 12.3 %all-to-all-start.3 = ((bf16[8,32,512]{2,1,0:T(8,128)(2,1)}), bf16[8,32,512]{2,1,0:T(8,128)(2,1)S(1)}, u32[]{:S(2)}, u32[]{:S(2)}) async-start(bf16[8,32,512]{2,1,0:T(8,128)(2,1)} %broadcast_in_dim.142), calls=%async_computation.3 | async-start | bytes 524288 | tf_op jit(solution)/shard_map/all_to_all | solution.py:35
  142.8 3.7 %collective-permute-start.4 = (bf16[256,128]{1,0:T(8,128)(2,1)S(1)}, bf16[256,128]{1,0:T(8,128)(2,1)S(1)}, u32[]{:S(2)}, u32[]{:S(2)}) collective-permute-start(bf16[256,128]{1,0:T(8,128)(2,1)S(1)} %get-tuple-element.24), channel_id=1, source_target_pairs={{0,1},{1,2},{2,3},{3,0},{4,5},{5,6},{6,7},{7,4},{8,9},{9,10},{10,1... | collective-permute-start | bytes 196616 | tf_op jit(solution)/shard_map/ppermute | solution.py:105
  142.9 4.1 %collective-permute-start.6 = (bf16[256,128]{1,0:T(8,128)(2,1)S(1)}, bf16[256,128]{1,0:T(8,128)(2,1)S(1)}, u32[]{:S(2)}, u32[]{:S(2)}) collective-permute-start(bf16[256,128]{1,0:T(8,128)(2,1)S(1)} %get-tuple-element.25), channel_id=1, source_target_pairs={{0,3},{1,0},{2,1},{3,2},{4,7},{5,4},{6,5},{7,6},{8,11},{9,8},{10,9... | collective-permute-start | bytes 196616 | tf_op jit(solution)/shard_map/ppermute | solution.py:105
  144.6 4.6 %collective-permute-start.5 = (bf16[256,128]{1,0:T(8,128)(2,1)S(1)}, bf16[256,128]{1,0:T(8,128)(2,1)S(1)}, u32[]{:S(2)}, u32[]{:S(2)}) collective-permute-start(bf16[256,128]{1,0:T(8,128)(2,1)S(1)} %get-tuple-element.26), channel_id=1, source_target_pairs={{0,2},{1,3},{2,0},{3,1},{4,6},{5,7},{6,4},{7,5},{8,10},{9,11},{10,... | collective-permute-start | bytes 196616 | tf_op jit(solution)/shard_map/ppermute | solution.py:105
  149.9 13.1 %all-to-all-start.4 = ((f32[32,1,256]{2,1,0:T(1,128)}), f32[32,1,256]{2,1,0:T(1,128)S(1)}, u32[]{:S(2)}, u32[]{:S(2)}) async-start(f32[32,1,256]{2,1,0:T(1,128)} %broadcast_in_dim.143), calls=%async_computation.4 | async-start | bytes 65536 | tf_op jit(solution)/shard_map/all_to_all | solution.py:35
  155.6 7.5 %copy-start.15 = (f32[128]{0:T(128)S(1)}, f32[128]{0:T(128)}, u32[]{:S(2)}) copy-start(f32[128]{0:T(128)} %param.23) | copy-start | bytes 1540
  (4 other events, 9.2 us)
where the time goes:
time: 165 us; the launch traced here: 164 us
  waiting for transfers between devices  68.8 us (42%)
  starting transfers between devices  38.3 us (23%)
  local copies, waits for them, and re-layouts  18.3 us (11%)
  matrix products  15.7 us (10%)
  other arithmetic  14.1 us (9%)
  Pallas kernels  7.4 us (4%)
    ppermute x6, waiting for transfers between devices, shifted(): lax.ppermute(block, axis, [(i, (i + step) % size) for i in range(size)])  42.5 us
    all_to_all x3, starting transfers between devices, gather_rows(): lax.all_to_all(copies, axis, 0, 0, tiled=True)  15.1 us
    all_to_all x3, waiting for transfers between devices, gather_rows(): lax.all_to_all(copies, axis, 0, 0, tiled=True)  14.6 us
    all_to_all x2, starting transfers between devices, exchange(): return lax.all_to_all(blocks, axis, 0, 0, tiled=True)  10.9 us
    all_to_all x2, waiting for transfers between devices, exchange(): return lax.all_to_all(blocks, axis, 0, 0, tiled=True)  8.8 us
    pallas_call x1, Pallas kernels, write_rows(): pl.pallas_call(write_kernel, out_shape=(shape, shape), grid_spec=pltpu.Pr...  7.4 us
    ppermute x6, starting transfers between devices, shifted(): lax.ppermute(block, axis, [(i, (i + step) % size) for i in range(size)])  6.6 us
    broadcast_in_dim x3, local copies, waits for them, and re-layouts, fold_gather(): lax.dynamic_update_index_in_dim(held, arrived, (group + groups - step) %...  3.34 us
  transfers between devices with their start and end apart: 16, of which 11 were waited for; matrix products, arithmetic and copies ran while one was open for 24% of the time, Pallas kernels for 5%

commit v1 on v0

--- a/solution.py
+++ b/solution.py
@@ -2,6 +2,7 @@
 import jax.numpy as jnp
 from jax import lax
 from jax.experimental import pallas as pl
+from jax.experimental.layout import Layout, with_layout_constraint
 from jax.experimental.pallas import tpu as pltpu
 from jax.sharding import PartitionSpec as P
 
@@ -46,6 +47,10 @@
 def shifted(block, axis, step):
     size = lax.axis_size(axis)
     return lax.ppermute(block, axis, [(i, (i + step) % size) for i in range(size)])
+
+
+def row_major(array):
+    return with_layout_constraint(array, Layout(major_to_minor=tuple(range(array.ndim))))
 
 
 def fold_of(axis):
@@ -62,16 +67,20 @@
     half = lax.dynamic_index_in_dim(blocks, mine, 1, False)
     if fold > 1:
         arrived = lax.ppermute(
-            lax.dynamic_index_in_dim(blocks, 1 - mine, 1, False),
+            row_major(lax.dynamic_index_in_dim(blocks, 1 - mine, 1, False)),
             axis,
             [(i, i ^ 1) for i in range(size)],
         )
-        half = (half.astype(jnp.float32) + arrived.astype(jnp.float32)).astype(rows.dtype)
+        half = row_major(
+            (half.astype(jnp.float32) + row_major(arrived).astype(jnp.float32)).astype(rows.dtype)
+        )
     group = rank // fold
     total = lax.dynamic_index_in_dim(half, group, 0, False).astype(jnp.float32)
     for step in range(1, groups):
-        block = lax.dynamic_index_in_dim(half, (group + step) % groups, 0, False)
-        arrived = shifted(block, axis, step * fold)
+        block = row_major(
+            lax.dynamic_index_in_dim(half, (group + step) % groups, 0, False)
+        )
+        arrived = row_major(shifted(block, axis, step * fold))
         total = total + arrived.astype(jnp.float32)
     return total
 
@@ -85,13 +94,14 @@
     held = jnp.zeros((groups,) + rows.shape, rows.dtype)
     held = lax.dynamic_update_index_in_dim(held, rows, group, 0)
     for step in range(1, groups):
-        arrived = shifted(rows, axis, step * fold)
+        arrived = row_major(shifted(rows, axis, step * fold))
         held = lax.dynamic_update_index_in_dim(
             held, arrived, (group + groups - step) % groups, 0
         )
     if fold == 1:
         return held.reshape((size * rows.shape[0],) + rows.shape[1:])
-    other = lax.ppermute(held, axis, [(i, i ^ 1) for i in range(size)])
+    held = row_major(held)
+    other = row_major(lax.ppermute(held, axis, [(i, i ^ 1) for i in range(size)]))
     even = rank % 2 == 0
     both = jnp.stack([jnp.where(even, held, other), jnp.where(even, other, held)], axis=1)
     return both.reshape((size * rows.shape[0],) + rows.shape[1:])
@@ -115,49 +125,65 @@
     return total
 
 
-def write_kernel(starts, key_in, value_in, key_new, value_new, key_out, value_out):
-    seqs, span = key_in.shape[:2]
-    members = key_new.shape[1]
-    key_out[...] = key_in[...]
-    value_out[...] = value_in[...]
-    for local in range(seqs):
-        start = starts[pl.program_id(0) * seqs + local]
+def write_kernel(starts, cache, new, out, held, in_sems, out_sems):
+    seqs, span = cache.shape[:2]
+    members = new.shape[1]
+
+    def arriving(seq):
+        return pltpu.make_async_copy(cache.at[seq], held.at[seq], in_sems.at[seq])
+
+    def leaving(seq):
+        return pltpu.make_async_copy(held.at[seq], out.at[seq], out_sems.at[seq])
+
+    def begin(seq, carry):
+        arriving(seq).start()
+        return carry
+
+    def patch(seq, carry):
+        arriving(seq).wait()
+        start = starts[seq]
 
         @pl.when((start > -members) & (start < span))
         def _():
-            def place(member, carry):
+            for member in range(members):
                 spot = start + member
 
                 @pl.when((spot >= 0) & (spot < span))
                 def _():
-                    key_out[local, spot] = key_new[local, member]
-                    value_out[local, spot] = value_new[local, member]
-
-                return carry
-
-            lax.fori_loop(0, members, place, 0)
-
-
-def write_rows(starts, key_cache, value_cache, key_new, value_new):
-    num_seqs, span, heads, width = key_cache.shape
-    members = key_new.shape[1]
-    step = 2 if num_seqs % 2 == 0 else 1
-    cache_spec = pl.BlockSpec((step, span, heads, width), lambda s, starts: (s, 0, 0, 0))
-    new_spec = pl.BlockSpec((step, members, heads, width), lambda s, starts: (s, 0, 0, 0))
-    shape = jax.ShapeDtypeStruct(key_cache.shape, key_cache.dtype)
+                    held[seq, spot] = new[seq, member]
+
+        leaving(seq).start()
+        return carry
+
+    def finish(seq, carry):
+        leaving(seq).wait()
+        return carry
+
+    lax.fori_loop(0, seqs, begin, 0)
+    lax.fori_loop(0, seqs, patch, 0)
+    lax.fori_loop(0, seqs, finish, 0)
+
+
+def write_rows(starts, cache, new):
+    num_seqs = cache.shape[0]
     return pl.pallas_call(
         write_kernel,
-        out_shape=(shape, shape),
-        grid_spec=pltpu.PrefetchScalarGridSpec(
-            num_scalar_prefetch=1,
-            grid=(num_seqs // step,),
-            in_specs=[cache_spec, cache_spec, new_spec, new_spec],
-            out_specs=(cache_spec, cache_spec),
+        out_shape=jax.ShapeDtypeStruct(cache.shape, cache.dtype),
+        in_specs=[
+            pl.BlockSpec(memory_space=pltpu.SMEM),
+            pl.BlockSpec(memory_space=pl.ANY),
+            pl.BlockSpec(memory_space=pltpu.VMEM),
+        ],
+        out_specs=pl.BlockSpec(memory_space=pl.ANY),
+        scratch_shapes=[
+            pltpu.VMEM(cache.shape, cache.dtype),
+            pltpu.SemaphoreType.DMA((num_seqs,)),
+            pltpu.SemaphoreType.DMA((num_seqs,)),
+        ],
+        cost_estimate=pl.CostEstimate(
+            flops=8 * cache.size, bytes_accessed=4 * cache.size, transcendentals=0
         ),
-        cost_estimate=pl.CostEstimate(
-            flops=8 * key_cache.size, bytes_accessed=8 * key_cache.size, transcendentals=0
-        ),
-    )(starts, key_cache, value_cache, key_new, value_new)
+    )(starts, cache, new)
 
 
 def ancestry(parent_ids, members):
@@ -260,8 +286,8 @@
         ],
         axis=1,
     )
-    own = fold_sum(sent, "kv").astype(jnp.bfloat16)
-    full = fold_gather(own, "kv")
+    own = row_major(fold_sum(row_major(sent), "kv").astype(jnp.bfloat16))
+    full = row_major(fold_gather(own, "kv"))
     own_last = unpack_lanes(own[:, 2 * head_width :], heads_local)
     last_rows_all = unpack_lanes(full[:, 2 * head_width :], heads_local)
     last_cum = last_rows_all.reshape(num_seqs, proposals, heads_local)[:, 0]
@@ -273,7 +299,6 @@
     live = (positions[None, :] < valid[:, None])[:, None, None, :]
     score = (
         jnp.einsum("bihd,bkhd->bihk", query, key_cache, preferred_element_type=jnp.float32) * scale
-        + path[..., None]
         - jnp.swapaxes(cum_cache, 1, 2)[:, None]
     )
     block_max = jnp.max(jnp.where(live, score, floor_value), axis=-1)
@@ -331,8 +356,9 @@
         preferred_element_type=jnp.float32,
     )
     logs_in = unpack_lanes(blocks_in[:, :, head_width:], heads_local)
-    cache_max = jnp.max(logs_in, axis=0)
-    shares = jnp.exp(logs_in - cache_max[None])
+    row_max = jnp.max(logs_in, axis=0)
+    shares = jnp.exp(logs_in - row_max[None])
+    cache_max = row_max + own_path.reshape(rows_local, heads_local)
     cache_total = jnp.sum(shares, axis=0)
     cache_values = jnp.sum(
         blocks_in[:, :, :head_width]
@@ -354,9 +380,8 @@
     mixed_part = jnp.dot(attended, w_out, preferred_element_type=jnp.float32)
     mixed_sum = scatter_columns(mixed_part.astype(jnp.bfloat16), "tp")
     own_squares = jnp.sum(mixed_sum * mixed_sum, axis=1)
-    squares = jnp.sum(
-        gather_rows(own_squares[None], ("kv", "tp")), axis=0
-    )
+    squares_in = gather_rows(own_squares[None], ("kv", "tp"))
+    squares = jnp.sum(squares_in, axis=0)
     mixed = (mixed_sum * lax.rsqrt(squares / model_width + epsilon)[:, None] * gain_post).astype(
         jnp.bfloat16
     )
@@ -364,9 +389,9 @@
     relative = positions[None, :] - valid[:, None]
     select = relative[:, :, None] == jnp.arange(proposals, dtype=jnp.int32)[None, None, :]
     written = (relative >= 0) & (relative < proposals)
-    key_out, value_out = write_rows(
-        valid - kv_rank * span, key_cache, value_cache, key_new, value_new
-    )
+    starts = valid - kv_rank * span
+    key_out = write_rows(starts, key_cache, key_new)
+    value_out = write_rows(starts, value_cache, value_new)
     cum_new = last_cum[:, None, :] + path
     placed_cum = jnp.einsum(
         "bkj,bjh->bkh", select.astype(jnp.float32), cum_new, precision=lax.Precision.HIGHEST

time: 165 us -> 117 us (0.71)
  waiting for transfers between devices: 68.8 us -> 32.1 us
  local copies, waits for them, and re-layouts: 18.3 us -> 12.9 us
  starting transfers between devices: 38.3 us -> 35.2 us
  other arithmetic: 14.1 us -> 12.3 us
    ppermute x6, waiting for transfers between devices: 42.5 us -> 6.31 us  [shifted(): lax.ppermute(block, axis, [(i, (i + step) % size) for i in range(size)])]
    all_to_all x3, starting transfers between devices: 15.1 us -> 9.52 us  [gather_rows(): lax.all_to_all(copies, axis, 0, 0, tiled=True)]
    broadcast_in_dim x4 -> x0, local copies, waits for them, and re-layouts: 3.49 us -> none  [the longest x3 3.34 us: fold_gather(): lax.dynamic_update_index_in_dim(held, arrived, (group + groups - step) %...]
    ppermute x6, starting transfers between devices: 6.6 us -> 9.15 us  [shifted(): lax.ppermute(block, axis, [(i, (i + step) % size) for i in range(size)])]
    pallas_call x1 -> x2, Pallas kernels: 7.4 us -> 7.08 us  [write_rows(): pl.pallas_call(write_kernel, out_shape=jax.ShapeDtypeStruct(cache.shape,...]
  transfers between devices with their start and end apart: 16 -> 16, of which waited for: 11 -> 8; matrix products, arithmetic and copies ran while one was open for 24% -> 26% of each run, Pallas kernels for 5% -> 6%
where the time goes in v1:
time: 117 us; the launch traced here: 116 us
  starting transfers between devices  35.2 us (30%)
  waiting for transfers between devices  32.1 us (27%)
  matrix products  15.1 us (13%)
  local copies, waits for them, and re-layouts  12.9 us (11%)
  other arithmetic  12.3 us (11%)
  Pallas kernels  7.08 us (6%)
  between operations  1.36 us (1%)
    all_to_all x3, waiting for transfers between devices, gather_rows(): lax.all_to_all(copies, axis, 0, 0, tiled=True)  13.7 us
    all_to_all x2, starting transfers between devices, exchange(): return lax.all_to_all(blocks, axis, 0, 0, tiled=True)  10.7 us
    all_to_all x3, starting transfers between devices, gather_rows(): lax.all_to_all(copies, axis, 0, 0, tiled=True)  9.52 us
    ppermute x6, starting transfers between devices, shifted(): lax.ppermute(block, axis, [(i, (i + step) % size) for i in range(size)])  9.15 us
    all_to_all x2, waiting for transfers between devices, exchange(): return lax.all_to_all(blocks, axis, 0, 0, tiled=True)  8.33 us
    pallas_call x2, Pallas kernels, write_rows(): pl.pallas_call(write_kernel, out_shape=jax.ShapeDtypeStruct(cache.shape,...  7.08 us
    ppermute x6, waiting for transfers between devices, shifted(): lax.ppermute(block, axis, [(i, (i + step) % size) for i in range(size)])  6.31 us
    ppermute x3, waiting for transfers between devices, scatter_columns(): lax.ppermute(lax.dynamic_slice_in_dim(part, (rank + step) % size * width,...  3.8 us
  transfers between devices with their start and end apart: 16, of which 8 were waited for; matrix products, arithmetic and copies ran while one was open for 26% of the time, Pallas kernels for 6%

profile of v1, /device:TPU:0, one launch (start us, length us, event | category | flops | bytes accessed | tf_op | source)
XLA Modules:
  0.0 115.9 jit_solution(11505779328369585803)
XLA Ops:
  0.7 2.2 %fusion = f32[16,16]{1,0:T(8,128)S(1)} fusion(bf16[16,16,4096]{2,1,0:T(8,128)(2,1)} %param.15), kind=kLoop, calls=%fused_computation.2 | loop fusion | flops 3145472 | bytes 2098176 | tf_op jit(solution)/shard_map/reduce_sum | solution.py:241
  2.9 0.8 dynamic_slice.54
  3.8 1.0 convolution_convert_fusion.3
  4.9 7.3 %all-to-all-start = ((bf16[8,32,512]{2,1,0:T(8,128)(2,1)}), bf16[8,32,512]{2,1,0:T(8,128)(2,1)S(1)}, u32[]{:S(2)}, u32[]{:S(2)}) async-start(bf16[8,32,512]{2,1,0:T(8,128)(2,1)} %bitcast.1), calls=%async_computation | async-start | bytes 524288 | tf_op jit(solution)/shard_map/all_to_all | solution.py:44
  13.9 2.0 %convolution_convert_fusion.1 = bf16[256,512]{1,0:T(8,128)(2,1)} fusion(bf16[256,512]{1,0:T(8,128)(2,1)S(1)} %bitcast.128, bf16[512,512]{1,0:T(8,128)(2,1)} %param.19), kind=kOutput, calls=%fused_computation.15 | convolution fusion | flops 134348800 | bytes 1048576 | tf_op jit(solution)/shard_map/dot_general | solution.py:260
  16.0 2.0 %convolution_convert_fusion.2 = bf16[256,512]{1,0:T(8,128)(2,1)} fusion(bf16[256,512]{1,0:T(8,128)(2,1)S(1)} %bitcast.129, bf16[512,512]{1,0:T(8,128)(2,1)} %param.18), kind=kOutput, calls=%fused_computation.16 | convolution fusion | flops 134348800 | bytes 1048576 | tf_op jit(solution)/shard_map/dot_general | solution.py:259
  18.0 1.1 fusion.30
  19.8 2.0 %collective-permute-start = (bf16[4,32,1152]{2,1,0:T(8,128)(2,1)}, bf16[4,32,1152]{2,1,0:T(8,128)(2,1)}, u32[]{:S(2)}, u32[]{:S(2)}) collective-permute-start(bf16[4,32,1152]{2,1,0:T(8,128)(2,1)} %dynamic-slice_bitcast_fusion), channel_id=1, source_target_pairs={{0,4},{4,0},{8,12},{12,8},{16,20},{20,16},{24,28},{28,24},{1,5},{5... | collective-permute-start | bytes 884744 | tf_op jit(solution)/shard_map/ppermute | solution.py:69
  21.9 2.7 %fusion.2 = bf16[16,16,4096]{2,1,0:T(8,128)(2,1)} fusion(bf16[16,16,4096]{2,1,0:T(8,128)(2,1)S(1)} %copy-done.1, f32[4096]{0:T(1024)} %param.16, f32[16,16]{1,0:T(8,128)S(1)} %add_rsqrt_fusion), kind=kLoop, calls=%fused_computation.4 | loop fusion | flops 4194304 | bytes 4211712 | tf_op jit(solution)/shard_map/convert_element_type | solution.py:258
  25.8 2.3 %fusion.74 = f32[256,4]{0,1:T(4,128)S(1)} fusion(bf16[256,4096]{1,0:T(8,128)(2,1)} %bitcast.126, bf16[4096,16]{0,1:T(8,128)(2,1)} %param.20, s32[]{:T(128)S(6)} %select_n.159, f32[4]{0:T(128)S(1)} %dynamic_slice.56), kind=kOutput, calls=%fused_computation.142 | convolution fusion | flops 8397824 | bytes 2134036 | tf_op jit(solution)/shard_map/dot_general | solution.py:264
  30.5 1.0 fusion.31
  31.6 3.3 %collective-permute-start.3 = (bf16[32,1152]{1,0:T(8,128)(2,1)S(1)}, bf16[32,1152]{1,0:T(8,128)(2,1)S(1)}, u32[]{:S(2)}, u32[]{:S(2)}) collective-permute-start(bf16[32,1152]{1,0:T(8,128)(2,1)S(1)} %get-tuple-element.21), channel_id=1, source_target_pairs={{0,24},{4,28},{8,0},{12,4},{16,8},{20,12},{24,16},{28,20},{1,25},{... | collective-permute-start | bytes 221192 | tf_op jit(solution)/shard_map/ppermute | solution.py:49
  34.9 1.1 collective-permute-start.1
  37.2 4.1 %collective-permute-done.2 = bf16[32,1152]{1,0:T(8,128)(2,1)S(1)} collective-permute-done((bf16[32,1152]{1,0:T(8,128)(2,1)S(1)}, bf16[32,1152]{1,0:T(8,128)(2,1)S(1)}, u32[]{:S(2)}, u32[]{:S(2)}) %collective-permute-start.2) | collective-permute-done | bytes 73760 | tf_op jit(solution)/shard_map/ppermute | solution.py:49
  42.2 2.3 %collective-permute-start.8 = (bf16[32,1152]{1,0:T(8,128)(2,1)S(1)}, bf16[32,1152]{1,0:T(8,128)(2,1)S(1)}, u32[]{:S(2)}, u32[]{:S(2)}) collective-permute-start(bf16[32,1152]{1,0:T(8,128)(2,1)S(1)} %get-tuple-element.5), channel_id=1, source_target_pairs={{0,16},{4,20},{8,24},{12,28},{16,0},{20,4},{24,8},{28,12},{1,17},{... | collective-permute-start | bytes 221192 | tf_op jit(solution)/shard_map/ppermute | solution.py:49
  44.6 2.3 %collective-permute-start.9 = (bf16[32,1152]{1,0:T(8,128)(2,1)S(1)}, bf16[32,1152]{1,0:T(8,128)(2,1)S(1)}, u32[]{:S(2)}, u32[]{:S(2)}) collective-permute-start(bf16[32,1152]{1,0:T(8,128)(2,1)S(1)} %get-tuple-element.5), channel_id=1, source_target_pairs={{0,24},{4,28},{8,0},{12,4},{16,8},{20,12},{24,16},{28,20},{1,25},{... | collective-permute-start | bytes 221192 | tf_op jit(solution)/shard_map/ppermute | solution.py:49
  46.9 1.6 %collective-permute-done.7 = bf16[32,1152]{1,0:T(8,128)(2,1)S(1)} collective-permute-done((bf16[32,1152]{1,0:T(8,128)(2,1)S(1)}, bf16[32,1152]{1,0:T(8,128)(2,1)S(1)}, u32[]{:S(2)}, u32[]{:S(2)}) %collective-permute-start.7) | collective-permute-done | bytes 73760 | tf_op jit(solution)/shard_map/ppermute | solution.py:49
  49.3 3.4 %all-to-all-start.1 = ((bf16[8,32,512]{2,1,0:T(8,128)(2,1)}), bf16[8,32,512]{2,1,0:T(8,128)(2,1)S(1)}, u32[]{:S(2)}, u32[]{:S(2)}) async-start(bf16[8,32,512]{2,1,0:T(8,128)(2,1)} %broadcast_in_dim.131), calls=%async_computation.1 | async-start | bytes 524288 | tf_op jit(solution)/shard_map/all_to_all | solution.py:36
  52.8 2.0 %collective-permute-start.10 = (bf16[4,32,1152]{2,1,0:T(8,128)(2,1)S(1)}, bf16[4,32,1152]{2,1,0:T(8,128)(2,1)S(1)}, u32[]{:S(2)}, u32[]{:S(2)}) collective-permute-start(bf16[4,32,1152]{2,1,0:T(8,128)(2,1)S(1)} %bitcast_dynamic-update-slice_fusion), channel_id=1, source_target_pairs={{0,4},{4,0},{8,12},{12,8},{16,20},{20,16},{24,28},{28,24},{1,5},{5... | collective-permute-start | bytes 884744 | tf_op jit(solution)/shard_map/ppermute | solution.py:104
  55.4 5.6 %all-to-all-done.1 = bf16[8,32,512]{2,1,0:T(8,128)(2,1)S(1)} async-done(((bf16[8,32,512]{2,1,0:T(8,128)(2,1)}), bf16[8,32,512]{2,1,0:T(8,128)(2,1)S(1)}, u32[]{:S(2)}, u32[]{:S(2)}) %all-to-all-start.1) | async-done | bytes 262176 | tf_op jit(solution)/shard_map/all_to_all | solution.py:36
  61.7 2.2 %select_reduce_fusion = (f32[16,16,4]{1,2,0:T(4,128)S(1)}, f32[16,16,4,128]{3,1,2,0:T(8,128)S(1)}) fusion(pred[16,128]{1,0:T(8,128)(4,1)} %get-tuple-element.34, f32[16,4,128]{2,1,0:T(4,128)} %bitcast.143, bf16[16,128,4,128]{3,2,1,0:T(4,128)(2,1)S(1)} %copy-done.2, bf16[16,16,4,128]{3,2,1,0:T(4,128)(2,1)} %reshape_reshape.3), kind=kOutput, calls=%fused_computation.39 | convolution fusion | flops 34077696 | bytes 2922496 | tf_op jit(solution)/shard_map/bihd,bkhd->bihk/dot_general | solution.py:301
  65.6 2.5 %fusion.22 = bf16[16,16,4,128]{3,1,2,0:T(8,128)(2,1)S(1)} fusion(bf16[16,128,4,128]{3,2,1,0:T(4,128)(2,1)} %cache.3, f32[16,16,4,128]{3,1,2,0:T(8,128)} %copy-done.3, f32[16,16,4]{1,2,0:T(4,128)S(1)} %compare_select_fusion, f32[16,16,4]{1,2,0:T(4,128)S(1)} %get-tuple-element.36, pred[16,128]{1,0:T(8,128)(4,1)} %get-tuple-element.34), kind=kOutput, calls=%fused_computation.18 | convolution fusion | flops 34209792 | bytes 2893824 | tf_op jit(solution)/shard_map/bihk,bkhd->bihd/dot_general | solution.py:307
  69.1 3.4 %all-to-all-start.2 = ((bf16[8,32,640]{2,1,0:T(8,128)(2,1)}), bf16[8,32,640]{2,1,0:T(8,128)(2,1)S(1)}, u32[]{:S(2)}, u32[]{:S(2)}) async-start(bf16[8,32,640]{2,1,0:T(8,128)(2,1)} %pad_maximum_fusion.1), calls=%async_computation.2 | async-start | bytes 655360 | tf_op jit(solution)/shard_map/all_to_all | solution.py:44
  72.8 8.3 %all-to-all-done.2 = bf16[8,32,640]{2,1,0:T(8,128)(2,1)S(1)} async-done(((bf16[8,32,640]{2,1,0:T(8,128)(2,1)}), bf16[8,32,640]{2,1,0:T(8,128)(2,1)S(1)}, u32[]{:S(2)}, u32[]{:S(2)}) %all-to-all-start.2) | async-done | bytes 327712 | tf_op jit(solution)/shard_map/all_to_all | solution.py:44
  84.3 3.5 %all-to-all-start.3 = ((bf16[8,32,512]{2,1,0:T(8,128)(2,1)}), bf16[8,32,512]{2,1,0:T(8,128)(2,1)S(1)}, u32[]{:S(2)}, u32[]{:S(2)}) async-start(bf16[8,32,512]{2,1,0:T(8,128)(2,1)} %broadcast_in_dim.141), calls=%async_computation.3 | async-start | bytes 524288 | tf_op jit(solution)/shard_map/all_to_all | solution.py:36
  87.9 8.1 %all-to-all-done.3 = bf16[8,32,512]{2,1,0:T(8,128)(2,1)S(1)} async-done(((bf16[8,32,512]{2,1,0:T(8,128)(2,1)}), bf16[8,32,512]{2,1,0:T(8,128)(2,1)S(1)}, u32[]{:S(2)}, u32[]{:S(2)}) %all-to-all-start.3) | async-done | bytes 262176 | tf_op jit(solution)/shard_map/all_to_all | solution.py:36
  96.4 1.5 %collective-permute-start.5 = (bf16[256,128]{1,0:T(8,128)(2,1)S(1)}, bf16[256,128]{1,0:T(8,128)(2,1)S(1)}, u32[]{:S(2)}, u32[]{:S(2)}) collective-permute-start(bf16[256,128]{1,0:T(8,128)(2,1)S(1)} %get-tuple-element.24), channel_id=1, source_target_pairs={{0,2},{1,3},{2,0},{3,1},{4,6},{5,7},{6,4},{7,5},{8,10},{9,11},{10,... | collective-permute-start | bytes 196616 | tf_op jit(solution)/shard_map/ppermute | solution.py:115
  98.4 3.7 %collective-permute-done.5 = bf16[256,128]{1,0:T(8,128)(2,1)S(1)} collective-permute-done((bf16[256,128]{1,0:T(8,128)(2,1)S(1)}, bf16[256,128]{1,0:T(8,128)(2,1)S(1)}, u32[]{:S(2)}, u32[]{:S(2)}) %collective-permute-start.5) | collective-permute-done | bytes 65568 | tf_op jit(solution)/shard_map/ppermute | solution.py:115
  103.0 2.6 %all-to-all-start.4 = ((f32[32,1,256]{2,1,0:T(1,128)}), f32[32,1,256]{2,1,0:T(1,128)S(1)}, u32[]{:S(2)}, u32[]{:S(2)}) async-start(f32[32,1,256]{2,1,0:T(1,128)} %broadcast_in_dim.142), calls=%async_computation.4 | async-start | bytes 65536 | tf_op jit(solution)/shard_map/all_to_all | solution.py:36
  105.6 0.9 convolution_select_fusion
  108.0 3.5 %shard_map.174 = bf16[16,128,4,128]{3,2,1,0:T(4,128)(2,1)} custom-call(s32[16]{0:T(128)} %get-tuple-element.6.starts, bf16[16,128,4,128]{3,2,1,0:T(4,128)(2,1)} %cache.2, bf16[16,16,4,128]{3,2,1,0:T(4,128)(2,1)} %reshape.289.new), custom_call_target="tpu_custom_call" | custom-call | flops 8388608 | bytes 4194304 | tf_op jit(solution)/shard_map/pallas_call | solution.py:169
  111.5 3.5 %shard_map.175 = bf16[16,128,4,128]{3,2,1,0:T(4,128)(2,1)} custom-call(s32[16]{0:T(128)} %get-tuple-element.6.starts, bf16[16,128,4,128]{3,2,1,0:T(4,128)(2,1)} %cache.3, bf16[16,16,4,128]{3,2,1,0:T(4,128)(2,1)} %reshape.290.new), custom_call_target="tpu_custom_call" | custom-call | flops 8388608 | bytes 4194304 | tf_op jit(solution)/shard_map/pallas_call | solution.py:169
  (160 shorter events, 20.4 us)
Async XLA Ops:
  0.7 11.5 %copy-start.21 = (s32[16]{0:T(128)S(1)}, s32[16]{0:T(128)}, u32[]{:S(2)}) copy-start(s32[16]{0:T(128)} %param.27) | copy-start | bytes 196
  0.7 11.5 %copy-start.22 = (s32[16]{0:T(128)S(1)}, s32[16]{0:T(128)}, u32[]{:S(2)}) copy-start(s32[16]{0:T(128)} %param.28) | copy-start | bytes 196
  0.7 12.7 %copy-start.7 = (f32[16,128,4]{1,2,0:T(4,128)S(1)}, f32[16,128,4]{1,2,0:T(4,128)}, u32[]{:S(2)}) copy-start(f32[16,128,4]{1,2,0:T(4,128)} %param.26) | copy-start | bytes 98308
  4.9 43.6 %all-to-all-start = ((bf16[8,32,512]{2,1,0:T(8,128)(2,1)}), bf16[8,32,512]{2,1,0:T(8,128)(2,1)S(1)}, u32[]{:S(2)}, u32[]{:S(2)}) async-start(bf16[8,32,512]{2,1,0:T(8,128)(2,1)} %bitcast.1), calls=%async_computation | async-start | bytes 524288 | tf_op jit(solution)/shard_map/all_to_all | solution.py:44
  19.8 10.7 %collective-permute-start = (bf16[4,32,1152]{2,1,0:T(8,128)(2,1)}, bf16[4,32,1152]{2,1,0:T(8,128)(2,1)}, u32[]{:S(2)}, u32[]{:S(2)}) collective-permute-start(bf16[4,32,1152]{2,1,0:T(8,128)(2,1)} %dynamic-slice_bitcast_fusion), channel_id=1, source_target_pairs={{0,4},{4,0},{8,12},{12,8},{16,20},{20,16},{24,28},{28,24},{1,5},{5... | collective-permute-start | bytes 884744 | tf_op jit(solution)/shard_map/ppermute | solution.py:69
  24.6 5.3 %copy-start.15 = (s32[16]{0:T(128)S(1)}, s32[16]{0:T(128)}, u32[]{:S(2)}) copy-start(s32[16]{0:T(128)} %copy-done.14) | copy-start | bytes 196
  24.6 5.3 %copy-start.19 = (s32[128]{0:T(128)S(1)}, s32[128]{0:T(128)}, u32[]{:S(2)}) copy-start(s32[128]{0:T(128)} %copy-done.18) | copy-start | bytes 1540
  31.6 30.2 %copy-start.2 = (bf16[16,128,4,128]{3,2,1,0:T(4,128)(2,1)S(1)}, bf16[16,128,4,128]{3,2,1,0:T(4,128)(2,1)}, u32[]{:S(2)}) copy-start(bf16[16,128,4,128]{3,2,1,0:T(4,128)(2,1)} %cache.2) | copy-start | bytes 6291460
  31.6 5.6 %collective-permute-start.3 = (bf16[32,1152]{1,0:T(8,128)(2,1)S(1)}, bf16[32,1152]{1,0:T(8,128)(2,1)S(1)}, u32[]{:S(2)}, u32[]{:S(2)}) collective-permute-start(bf16[32,1152]{1,0:T(8,128)(2,1)S(1)} %get-tuple-element.21), channel_id=1, source_target_pairs={{0,24},{4,28},{8,0},{12,4},{16,8},{20,12},{24,16},{28,20},{1,25},{... | collective-permute-start | bytes 221192 | tf_op jit(solution)/shard_map/ppermute | solution.py:49
  34.9 6.5 %collective-permute-start.2 = (bf16[32,1152]{1,0:T(8,128)(2,1)S(1)}, bf16[32,1152]{1,0:T(8,128)(2,1)S(1)}, u32[]{:S(2)}, u32[]{:S(2)}) collective-permute-start(bf16[32,1152]{1,0:T(8,128)(2,1)S(1)} %get-tuple-element.20), channel_id=1, source_target_pairs={{0,16},{4,20},{8,24},{12,28},{16,0},{20,4},{24,8},{28,12},{1,17},{... | collective-permute-start | bytes 221192 | tf_op jit(solution)/shard_map/ppermute | solution.py:49
  34.9 6.5 %collective-permute-start.1 = (bf16[32,1152]{1,0:T(8,128)(2,1)S(1)}, bf16[32,1152]{1,0:T(8,128)(2,1)S(1)}, u32[]{:S(2)}, u32[]{:S(2)}) collective-permute-start(bf16[32,1152]{1,0:T(8,128)(2,1)S(1)} %get-tuple-element.19), channel_id=1, source_target_pairs={{0,8},{4,12},{8,16},{12,20},{16,24},{20,28},{24,0},{28,4},{1,9},{5... | collective-permute-start | bytes 221192 | tf_op jit(solution)/shard_map/ppermute | solution.py:49
  41.5 7.0 %collective-permute-start.7 = (bf16[32,1152]{1,0:T(8,128)(2,1)S(1)}, bf16[32,1152]{1,0:T(8,128)(2,1)S(1)}, u32[]{:S(2)}, u32[]{:S(2)}) collective-permute-start(bf16[32,1152]{1,0:T(8,128)(2,1)S(1)} %get-tuple-element.5), channel_id=1, source_target_pairs={{0,8},{4,12},{8,16},{12,20},{16,24},{20,28},{24,0},{28,4},{1,9},{5... | collective-permute-start | bytes 221192 | tf_op jit(solution)/shard_map/ppermute | solution.py:49
  42.2 10.5 %collective-permute-start.8 = (bf16[32,1152]{1,0:T(8,128)(2,1)S(1)}, bf16[32,1152]{1,0:T(8,128)(2,1)S(1)}, u32[]{:S(2)}, u32[]{:S(2)}) collective-permute-start(bf16[32,1152]{1,0:T(8,128)(2,1)S(1)} %get-tuple-element.5), channel_id=1, source_target_pairs={{0,16},{4,20},{8,24},{12,28},{16,0},{20,4},{24,8},{28,12},{1,17},{... | collective-permute-start | bytes 221192 | tf_op jit(solution)/shard_map/ppermute | solution.py:49
  44.6 8.2 %collective-permute-start.9 = (bf16[32,1152]{1,0:T(8,128)(2,1)S(1)}, bf16[32,1152]{1,0:T(8,128)(2,1)S(1)}, u32[]{:S(2)}, u32[]{:S(2)}) collective-permute-start(bf16[32,1152]{1,0:T(8,128)(2,1)S(1)} %get-tuple-element.5), channel_id=1, source_target_pairs={{0,24},{4,28},{8,0},{12,4},{16,8},{20,12},{24,16},{28,20},{1,25},{... | collective-permute-start | bytes 221192 | tf_op jit(solution)/shard_map/ppermute | solution.py:49
  49.3 11.7 %all-to-all-start.1 = ((bf16[8,32,512]{2,1,0:T(8,128)(2,1)}), bf16[8,32,512]{2,1,0:T(8,128)(2,1)S(1)}, u32[]{:S(2)}, u32[]{:S(2)}) async-start(bf16[8,32,512]{2,1,0:T(8,128)(2,1)} %broadcast_in_dim.131), calls=%async_computation.1 | async-start | bytes 524288 | tf_op jit(solution)/shard_map/all_to_all | solution.py:36
  52.8 19.8 %collective-permute-start.10 = (bf16[4,32,1152]{2,1,0:T(8,128)(2,1)S(1)}, bf16[4,32,1152]{2,1,0:T(8,128)(2,1)S(1)}, u32[]{:S(2)}, u32[]{:S(2)}) collective-permute-start(bf16[4,32,1152]{2,1,0:T(8,128)(2,1)S(1)} %bitcast_dynamic-update-slice_fusion), channel_id=1, source_target_pairs={{0,4},{4,0},{8,12},{12,8},{16,20},{20,16},{24,28},{28,24},{1,5},{5... | collective-permute-start | bytes 884744 | tf_op jit(solution)/shard_map/ppermute | solution.py:104
  69.1 12.0 %all-to-all-start.2 = ((bf16[8,32,640]{2,1,0:T(8,128)(2,1)}), bf16[8,32,640]{2,1,0:T(8,128)(2,1)S(1)}, u32[]{:S(2)}, u32[]{:S(2)}) async-start(bf16[8,32,640]{2,1,0:T(8,128)(2,1)} %pad_maximum_fusion.1), calls=%async_computation.2 | async-start | bytes 655360 | tf_op jit(solution)/shard_map/all_to_all | solution.py:44
  72.5 9.0 %copy-start.11 = (f32[256,4]{0,1:T(4,128)S(1)}, f32[256,4]{0,1:T(4,128)}, u32[]{:S(2)}) copy-start(f32[256,4]{0,1:T(4,128)} %reshape.277) | copy-start | bytes 12292
  72.5 9.2 %copy-start.6 = (pred[2,16,16]{1,2,0:T(8,128)(4,1)S(1)}, pred[2,16,16]{1,2,0:T(8,128)(4,1)}, u32[]{:S(2)}) copy-start(pred[2,16,16]{1,2,0:T(8,128)(4,1)} %copy.220) | copy-start | bytes 1540
  72.6 9.2 %copy-start.9 = (bf16[2,16,4,128]{3,2,1,0:T(4,128)(2,1)S(1)}, bf16[2,16,4,128]{3,2,1,0:T(4,128)(2,1)}, u32[]{:S(2)}) copy-start(bf16[2,16,4,128]{3,2,1,0:T(4,128)(2,1)} %reshape.282) | copy-start | bytes 98308
  72.6 9.1 %copy-start.10 = (bf16[2,16,1,4,128]{4,3,2,1,0:T(4,128)(2,1)S(1)}, bf16[2,16,1,4,128]{4,3,2,1,0:T(4,128)(2,1)}, u32[]{:S(2)}) copy-start(bf16[2,16,1,4,128]{4,3,2,1,0:T(4,128)(2,1)} %get-tuple-element.26) | copy-start | bytes 98308
  72.6 9.1 %copy-start.16 = (f32[2,4,16]{2,1,0:T(4,128)S(1)}, f32[2,4,16]{2,1,0:T(4,128)}, u32[]{:S(2)}) copy-start(f32[2,4,16]{2,1,0:T(4,128)} %fusion.71) | copy-start | bytes 1540
  72.7 9.5 %copy-start.5 = (bf16[2,16,1,4,128]{4,3,2,1,0:T(4,128)(2,1)S(1)}, bf16[2,16,1,4,128]{4,3,2,1,0:T(4,128)(2,1)}, u32[]{:S(2)}) copy-start(bf16[2,16,1,4,128]{4,3,2,1,0:T(4,128)(2,1)} %get-tuple-element.25) | copy-start | bytes 98308
  83.0 13.0 %copy-start.4 = (bf16[512,512]{1,0:T(8,128)(2,1)S(1)}, bf16[512,512]{1,0:T(8,128)(2,1)}, u32[]{:S(2)}) copy-start(bf16[512,512]{1,0:T(8,128)(2,1)} %param.22) | copy-start | bytes 1572868
  84.2 21.3 %copy-start.8 = (f32[16,128,4]{1,2,0:T(4,128)S(1)}, f32[16,128,4]{1,2,0:T(4,128)}, u32[]{:S(2)}) copy-start(f32[16,128,4]{1,2,0:T(4,128)} %param.26) | copy-start | bytes 98308
  84.2 21.3 %copy-start.13 = (s32[16,128]{1,0:T(8,128)S(1)}, s32[16,128]{1,0:T(8,128)}, u32[]{:S(2)}) copy-start(s32[16,128]{1,0:T(8,128)} %broadcast_subtract_fusion) | copy-start | bytes 24580
  84.3 21.3 %copy-start.17 = (pred[16,128]{1,0:T(8,128)(4,1)S(1)}, pred[16,128]{1,0:T(8,128)(4,1)}, u32[]{:S(2)}) copy-start(pred[16,128]{1,0:T(8,128)(4,1)} %get-tuple-element.33) | copy-start | bytes 6148
  84.3 11.7 %all-to-all-start.3 = ((bf16[8,32,512]{2,1,0:T(8,128)(2,1)}), bf16[8,32,512]{2,1,0:T(8,128)(2,1)S(1)}, u32[]{:S(2)}, u32[]{:S(2)}) async-start(bf16[8,32,512]{2,1,0:T(8,128)(2,1)} %broadcast_in_dim.141), calls=%async_computation.3 | async-start | bytes 524288 | tf_op jit(solution)/shard_map/all_to_all | solution.py:36
  96.3 2.1 %collective-permute-start.6 = (bf16[256,128]{1,0:T(8,128)(2,1)S(1)}, bf16[256,128]{1,0:T(8,128)(2,1)S(1)}, u32[]{:S(2)}, u32[]{:S(2)}) collective-permute-start(bf16[256,128]{1,0:T(8,128)(2,1)S(1)} %get-tuple-element.23), channel_id=1, source_target_pairs={{0,3},{1,0},{2,1},{3,2},{4,7},{5,4},{6,5},{7,6},{8,11},{9,8},{10,9... | collective-permute-start | bytes 196616 | tf_op jit(solution)/shard_map/ppermute | solution.py:115
  96.4 5.7 %collective-permute-start.5 = (bf16[256,128]{1,0:T(8,128)(2,1)S(1)}, bf16[256,128]{1,0:T(8,128)(2,1)S(1)}, u32[]{:S(2)}, u32[]{:S(2)}) collective-permute-start(bf16[256,128]{1,0:T(8,128)(2,1)S(1)} %get-tuple-element.24), channel_id=1, source_target_pairs={{0,2},{1,3},{2,0},{3,1},{4,6},{5,7},{6,4},{7,5},{8,10},{9,11},{10,... | collective-permute-start | bytes 196616 | tf_op jit(solution)/shard_map/ppermute | solution.py:115
  97.9 4.3 %collective-permute-start.4 = (bf16[256,128]{1,0:T(8,128)(2,1)S(1)}, bf16[256,128]{1,0:T(8,128)(2,1)S(1)}, u32[]{:S(2)}, u32[]{:S(2)}) collective-permute-start(bf16[256,128]{1,0:T(8,128)(2,1)S(1)} %get-tuple-element.22), channel_id=1, source_target_pairs={{0,1},{1,2},{2,3},{3,0},{4,5},{5,6},{6,7},{7,4},{8,9},{9,10},{10,1... | collective-permute-start | bytes 196616 | tf_op jit(solution)/shard_map/ppermute | solution.py:115
  103.0 12.1 %all-to-all-start.4 = ((f32[32,1,256]{2,1,0:T(1,128)}), f32[32,1,256]{2,1,0:T(1,128)S(1)}, u32[]{:S(2)}, u32[]{:S(2)}) async-start(f32[32,1,256]{2,1,0:T(1,128)} %broadcast_in_dim.142), calls=%async_computation.4 | async-start | bytes 65536 | tf_op jit(solution)/shard_map/all_to_all | solution.py:36
  (9 other events, 22.2 us)
